TPU v7x, 32 devices: a whole 2x2x4 slice. The times are simulated.
32 devices in a mesh: grp: 2 (over y), fs: 4 (over z), tp: 4 (over x, core).
Axes of the slice: x: 2, y: 2, z: 4, core: 2. Of those that a mesh axis runs over, the one named last changes fastest.
Arguments:
- tokens: bfloat16 [4096, 2048], P(('grp', 'fs', 'tp')), parts along dimension 0, may hold values from -12 to 12
- norm_gain: float32 [2048], replicated, may hold values from 0.1 to 1.9
- w_in: bfloat16 [2048, 8192], P('fs', 'tp'), may hold values from -0.125 to 0.125
- w_out: bfloat16 [8192, 2048], P('tp', 'fs'), may hold values from -0.0625 to 0.0625
Outputs:
- mixed: bfloat16 [4096, 2048], P(('grp', 'fs', 'tp')), parts along dimension 0
There are 2 independent parts, one for each index of `grp`. A program takes and returns all parts, laid end to end along the dimension named above; an argument that names none is the same for every part. Nothing has to cross between parts.
All inputs are finite; a program needn't handle non-finite values.
Results may differ from a plain program's by a relative error of at most 0.012.
Values may be sent and summed in bfloat16 or wider, within the bound.
A program may use at most 64 MiB of HBM per device.

v0:
```python
import jax
import jax.numpy as jnp
from jax import lax
from jax.sharding import PartitionSpec as P

EPS = 1e-06


def local(tokens, norm_gain, w_in, w_out):
    xf = tokens.astype(jnp.float32)
    scale = lax.rsqrt(jnp.mean(xf * xf, axis=-1, keepdims=True) + EPS)
    normed = (xf * scale * norm_gain).astype(jnp.bfloat16)
    group = lax.all_gather(normed, "tp", axis=0, tiled=True)
    pre = jnp.dot(
        group, lax.all_gather(w_in, "fs", axis=0, tiled=True), preferred_element_type=jnp.float32
    )
    hidden = jnp.square(jax.nn.relu(pre)).astype(jnp.bfloat16)
    terms = jnp.dot(
        hidden, lax.all_gather(w_out, "fs", axis=1, tiled=True), preferred_element_type=jnp.float32
    )
    summed = lax.psum_scatter(
        terms.astype(jnp.bfloat16), "tp", scatter_dimension=0, tiled=True
    ).astype(jnp.float32)
    return (xf + summed).astype(jnp.bfloat16)


def solution(mesh):
    in_specs = (P(("grp", "fs", "tp"), None), P(), P("fs", "tp"), P("tp", "fs"))
    out_specs = P(("grp", "fs", "tp"), None)
    return jax.shard_map(local, mesh=mesh, in_specs=in_specs, out_specs=out_specs, check_vma=False)
```

profile of v0, /device:TPU:0, one launch (start us, length us, event | category | flops | bytes accessed | tf_op | source)
XLA Modules:
  0.0 390.5 jit_solution(15908731586754024758)
XLA Ops:
  6.5 0.0 all-gather.4.cloned.1.call-start
  6.5 1.2 fusion
  7.8 2.0 fusion.2
  9.8 0.0 all-gather.4.cloned.1.call-update
  9.8 0.0 all-gather.6.cloned.1.call-start
  9.9 0.7 all-gather.6.cloned.1.call-update
  10.6 0.0 all-gather.8.cloned.1.call-start
  10.6 0.7 all-gather.8.cloned.1.call-update
  11.3 0.0 copy-start
  11.3 0.0 reduce-scatter.2.cloned.1.call-start
  11.4 23.9 %all-gather.4.cloned.1.call-done = bf16[512,2048]{1,0:T(8,128)(2,1)} async-done(((bf16[128,2048]{1,0:T(8,128)(2,1)}), bf16[512,2048]{1,0:T(8,128)(2,1)}) %all-gather.4.cloned.1.call-update) | async-done | bytes 2097168 | tf_op jit(solution)/shard_map/all_gather | solution.py:13
  35.3 151.2 %all-gather.6.cloned.1.call-done = bf16[2048,2048]{1,0:T(8,128)(2,1)} async-done(((bf16[512,2048]{1,0:T(8,128)(2,1)}), bf16[2048,2048]{1,0:T(8,128)(2,1)}) %all-gather.6.cloned.1.call-update) | async-done | bytes 8388624 | tf_op jit(solution)/shard_map/all_gather | solution.py:15
  186.5 149.4 %all-gather.8.cloned.1.call-done = bf16[2048,2048]{1,0:T(8,128)(2,1)} async-done(((bf16[2048,512]{1,0:T(8,128)(2,1)}), bf16[2048,2048]{1,0:T(8,128)(2,1)}) %all-gather.8.cloned.1.call-update) | async-done | bytes 8388624 | tf_op jit(solution)/shard_map/all_gather | solution.py:19
  335.9 16.5 %convolution_convert_fusion = bf16[512,2048]{1,0:T(8,128)(2,1)} fusion(bf16[2048,2048]{1,0:T(8,128)(2,1)} %all-gather.8.cloned.1.call-done, bf16[512,2048]{1,0:T(8,128)(2,1)} %all-gather.4.cloned.1.call-done, bf16[2048,2048]{1,0:T(8,128)(2,1)} %all-gather.6.cloned.1.call-done), kind=kOutput, calls=%fused_computation.1 | convolution fusion | flops 8594128896 | bytes 20971520 | tf_op jit(solution)/shard_map/dot_general | solution.py:18
  352.4 0.0 reduce-scatter.2.cloned.1.call-update
  352.4 29.5 %reduce-scatter.2.cloned.1.call-done = bf16[128,2048]{1,0:T(8,128)(2,1)} async-done(((bf16[512,2048]{1,0:T(8,128)(2,1)}), bf16[128,2048]{1,0:T(8,128)(2,1)}) %reduce-scatter.2.cloned.1.call-update) | async-done | bytes 524304 | tf_op jit(solution)/shard_map/reduce_scatter | solution.py:21
  382.0 0.0 copy-done
  382.0 2.0 fusion.3
  (1 shorter events, 0.0 us)
Async XLA Ops:
  6.5 28.7 %all-gather.4.cloned.1.call-start = ((), (), s32[]{:S(2)}) async-start(), calls=%async_computation.1 | async-start | bytes 2621440 | tf_op jit(solution)/shard_map/all_gather | solution.py:13
  9.8 176.7 %all-gather.6.cloned.1.call-start = ((), (), s32[]{:S(2)}) async-start(), calls=%async_computation.2 | async-start | bytes 10485760 | tf_op jit(solution)/shard_map/all_gather | solution.py:15
  10.6 325.3 %all-gather.8.cloned.1.call-start = ((), (), s32[]{:S(2)}) async-start(), calls=%async_computation.3 | async-start | bytes 10485760 | tf_op jit(solution)/shard_map/all_gather | solution.py:19
  11.3 370.6 %copy-start = (bf16[128,2048]{1,0:T(8,128)(2,1)S(1)}, bf16[128,2048]{1,0:T(8,128)(2,1)}, u32[]{:S(2)}) copy-start(bf16[128,2048]{1,0:T(8,128)(2,1)} %param.4) | copy-start | bytes 1572868
  11.3 370.6 %reduce-scatter.2.cloned.1.call-start = ((), (), s32[]{:S(2)}) async-start(), calls=%async_computation.4 | async-start | bytes 2621440 | tf_op jit(solution)/shard_map/reduce_scatter | solution.py:21
Sparse Core Ops, SparseCore 0:
  9.9 25.2 all-gather.3
  36.8 149.6 all-gather.5
  188.1 147.7 all-gather.7
  352.6 29.3 reduce-scatter.1
where the time goes:
time: 391 us; the launch traced here: 390 us
  waiting for transfers between devices  355 us (91%)
  matrix products  16.5 us (4%)
  between operations  13.1 us (3%)
  other arithmetic  5.23 us (1%)
    all_gather x1, waiting for transfers between devices, local(): lax.all_gather(w_in, 'fs', axis=0, tiled=True)  151 us
    all_gather x1, waiting for transfers between devices, local(): lax.all_gather(w_out, 'fs', axis=1, tiled=True)  149 us
    reduce_scatter x1, waiting for transfers between devices, local(): lax.psum_scatter(terms.astype(jnp.bfloat16), 'tp', scatter_dimension=0, t...  29.5 us
    all_gather x1, waiting for transfers between devices, local(): group = lax.all_gather(normed, 'tp', axis=0, tiled=True)  23.9 us
    dot_general x1, matrix products, local(): jnp.dot(hidden, lax.all_gather(w_out, 'fs', axis=1, tiled=True), preferre...  16.5 us
  transfers between devices with their start and end apart: 4, of which 4 were waited for; matrix products, arithmetic and copies ran while one was open for 0% of the time, Pallas kernels for 0%

commit v1 on v0

--- a/solution.py
+++ b/solution.py
@@ -10,7 +10,12 @@
     xf = tokens.astype(jnp.float32)
     scale = lax.rsqrt(jnp.mean(xf * xf, axis=-1, keepdims=True) + EPS)
     normed = (xf * scale * norm_gain).astype(jnp.bfloat16)
-    group = lax.all_gather(normed, "tp", axis=0, tiled=True)
+    ring = [normed]
+    for hop in range(3):
+        ring.append(lax.ppermute(ring[-1], "tp", [(dev, (dev + 1) % 4) for dev in range(4)]))
+    group = jnp.roll(
+        jnp.concatenate(ring[::-1], axis=0), (lax.axis_index("tp") + 1) * ring[0].shape[0], axis=0
+    )
     pre = jnp.dot(
         group, lax.all_gather(w_in, "fs", axis=0, tiled=True), preferred_element_type=jnp.float32
     )

time: 391 us -> 365 us (0.934)
  waiting for transfers between devices: 355 us -> 326 us
  local copies, waits for them, and re-layouts: 0.01 us -> 5.05 us
    all_gather x1, waiting for transfers between devices: 151 us -> 119 us  [local(): lax.all_gather(w_in, 'fs', axis=0, tiled=True)]
    ppermute x0 -> x3, waiting for transfers between devices: none -> 26 us  [local(): lax.ppermute(ring[-1], 'tp', [(dev, (dev + 1) % 4) for dev in range(4)])]
    all_gather x1 -> x0, waiting for transfers between devices: 23.9 us -> none  [local(): group = lax.all_gather(normed, 'tp', axis=0, tiled=True)]
    unnamed x2 -> x10, local copies, waits for them, and re-layouts: 0.01 us -> 5.05 us
  transfers between devices with their start and end apart: 4 -> 6, of which waited for: 4 -> 6; matrix products, arithmetic and copies ran while one was open for 0% -> 2% of each run, Pallas kernels for 0% -> 0%
where the time goes in v1:
time: 365 us
  waiting for transfers between devices  326 us (89%)
  matrix products  16.5 us (5%)
  between operations  13.1 us (4%)
  local copies, waits for them, and re-layouts  5.05 us (1%)
  other arithmetic  4.3 us (1%)
    all_gather x1, waiting for transfers between devices, local(): lax.all_gather(w_out, 'fs', axis=1, tiled=True)  149 us
    all_gather x1, waiting for transfers between devices, local(): lax.all_gather(w_in, 'fs', axis=0, tiled=True)  119 us
    reduce_scatter x1, waiting for transfers between devices, local(): lax.psum_scatter(terms.astype(jnp.bfloat16), 'tp', scatter_dimension=0, t...  29.5 us
    ppermute x3, waiting for transfers between devices, local(): lax.ppermute(ring[-1], 'tp', [(dev, (dev + 1) % 4) for dev in range(4)])  26 us
    dot_general x1, matrix products, local(): jnp.dot(hidden, lax.all_gather(w_out, 'fs', axis=1, tiled=True), preferre...  16.5 us
  transfers between devices with their start and end apart: 6, of which 6 were waited for; matrix products, arithmetic and copies ran while one was open for 2% of the time, Pallas kernels for 0%

profile of v1, /device:TPU:0, one launch (start us, length us, event | category | flops | bytes accessed | tf_op | source)
XLA Modules:
  0.0 365.2 jit_solution(8632855996958187565)
XLA Ops:
  6.5 0.7 all-gather.3.cloned.1.call-update
  7.3 0.0 all-gather.5.cloned.1.call-start
  7.3 0.7 all-gather.5.cloned.1.call-update
  8.0 0.0 reduce-scatter.2.cloned.1.call-start
  8.1 0.2 fusion.1
  8.3 0.2 fusion.3
  8.5 0.5 collective-permute-start
  9.0 8.8 %collective-permute-done = bf16[128,2048]{1,0:T(8,128)(2,1)S(1)} collective-permute-done((bf16[128,2048]{1,0:T(8,128)(2,1)S(1)}, bf16[128,2048]{1,0:T(8,128)(2,1)S(1)}, u32[]{:S(2)}, u32[]{:S(2)}) %collective-permute-start) | collective-permute-done | bytes 524320 | tf_op jit(solution)/shard_map/ppermute | solution.py:15
  17.8 8.6 %collective-permute-done.1 = bf16[128,2048]{1,0:T(8,128)(2,1)S(1)} collective-permute-done((bf16[128,2048]{1,0:T(8,128)(2,1)S(1)}, bf16[128,2048]{1,0:T(8,128)(2,1)S(1)}, u32[]{:S(2)}, u32[]{:S(2)}) %collective-permute-start.1) | collective-permute-done | bytes 524320 | tf_op jit(solution)/shard_map/ppermute | solution.py:15
  26.4 8.6 %collective-permute-done.2 = bf16[128,2048]{1,0:T(8,128)(2,1)S(1)} collective-permute-done((bf16[128,2048]{1,0:T(8,128)(2,1)S(1)}, bf16[128,2048]{1,0:T(8,128)(2,1)S(1)}, u32[]{:S(2)}, u32[]{:S(2)}) %collective-permute-start.2) | collective-permute-done | bytes 524320 | tf_op jit(solution)/shard_map/ppermute | solution.py:15
  35.0 0.8 constant_dynamic-update-slice_fusion.7
  35.9 0.8 constant_dynamic-update-slice_fusion.6
  36.7 0.8 constant_dynamic-update-slice_fusion.5
  37.5 1.0 constant_dynamic-update-slice_fusion.4
  38.5 0.8 constant_dynamic-update-slice_fusion.3
  39.3 0.8 constant_dynamic-update-slice_fusion.2
  40.2 0.8 constant_dynamic-update-slice_fusion.1
  41.0 1.0 constant_dynamic-update-slice_fusion
  42.0 119.3 %all-gather.3.cloned.1.call-done = bf16[2048,2048]{1,0:T(8,128)(2,1)} async-done(((bf16[512,2048]{1,0:T(8,128)(2,1)}), bf16[2048,2048]{1,0:T(8,128)(2,1)}) %all-gather.3.cloned.1.call-update) | async-done | bytes 8388624 | tf_op jit(solution)/shard_map/all_gather | solution.py:20
  161.3 149.4 %all-gather.5.cloned.1.call-done = bf16[2048,2048]{1,0:T(8,128)(2,1)} async-done(((bf16[2048,512]{1,0:T(8,128)(2,1)}), bf16[2048,2048]{1,0:T(8,128)(2,1)}) %all-gather.5.cloned.1.call-update) | async-done | bytes 8388624 | tf_op jit(solution)/shard_map/all_gather | solution.py:24
  310.7 16.5 %convolution_convert_fusion = bf16[512,2048]{1,0:T(8,128)(2,1)} fusion(bf16[2048,2048]{1,0:T(8,128)(2,1)} %all-gather.5.cloned.1.call-done, bf16[2048,2048]{1,0:T(8,128)(2,1)} %all-gather.3.cloned.1.call-done, bf16[1024,2048]{1,0:T(8,128)(2,1)} %constant_dynamic-update-slice_fusion, s32[]{:T(128)S(6)} %select_n.14), kind=kOutput, calls=%fused_computation.1 | convolution fusion | flops 8594128896 | bytes 20971524 | tf_op jit(solution)/shard_map/dot_general | solution.py:23
  327.2 0.0 reduce-scatter.2.cloned.1.call-update
  327.2 29.5 %reduce-scatter.2.cloned.1.call-done = bf16[128,2048]{1,0:T(8,128)(2,1)} async-done(((bf16[512,2048]{1,0:T(8,128)(2,1)}), bf16[128,2048]{1,0:T(8,128)(2,1)}) %reduce-scatter.2.cloned.1.call-update) | async-done | bytes 524304 | tf_op jit(solution)/shard_map/reduce_scatter | solution.py:26
  356.7 2.0 fusion.4
  (8 shorter events, 0.0 us)
Async XLA Ops:
  6.5 1.5 copy-start
  6.5 1.7 copy-start.1
  6.5 154.7 %all-gather.3.cloned.1.call-start = ((), (), s32[]{:S(2)}) async-start(), calls=%async_computation.1 | async-start | bytes 10485760 | tf_op jit(solution)/shard_map/all_gather | solution.py:20
  7.3 303.4 %all-gather.5.cloned.1.call-start = ((), (), s32[]{:S(2)}) async-start(), calls=%async_computation.2 | async-start | bytes 10485760 | tf_op jit(solution)/shard_map/all_gather | solution.py:24
  8.0 348.7 %reduce-scatter.2.cloned.1.call-start = ((), (), s32[]{:S(2)}) async-start(), calls=%async_computation.3 | async-start | bytes 2621440 | tf_op jit(solution)/shard_map/reduce_scatter | solution.py:26
  8.5 9.3 %collective-permute-start = (bf16[128,2048]{1,0:T(8,128)(2,1)S(1)}, bf16[128,2048]{1,0:T(8,128)(2,1)S(1)}, u32[]{:S(2)}, u32[]{:S(2)}) collective-permute-start(bf16[128,2048]{1,0:T(8,128)(2,1)S(1)} %fusion.3), channel_id=1, source_target_pairs={{0,1},{1,2},{2,3},{3,0},{4,5},{5,6},{6,7},{7,4},{8,9},{9,10},{10,1... | collective-permute-start | bytes 1572872 | tf_op jit(solution)/shard_map/ppermute | solution.py:15
  17.8 8.6 %collective-permute-start.1 = (bf16[128,2048]{1,0:T(8,128)(2,1)S(1)}, bf16[128,2048]{1,0:T(8,128)(2,1)S(1)}, u32[]{:S(2)}, u32[]{:S(2)}) collective-permute-start(bf16[128,2048]{1,0:T(8,128)(2,1)S(1)} %collective-permute-done), channel_id=1, source_target_pairs={{0,1},{1,2},{2,3},{3,0},{4,5},{5,6},{6,7},{7,4},{8,9},{9,10},{10,1... | collective-permute-start | bytes 1572872 | tf_op jit(solution)/shard_map/ppermute | solution.py:15
  26.4 8.6 %collective-permute-start.2 = (bf16[128,2048]{1,0:T(8,128)(2,1)S(1)}, bf16[128,2048]{1,0:T(8,128)(2,1)S(1)}, u32[]{:S(2)}, u32[]{:S(2)}) collective-permute-start(bf16[128,2048]{1,0:T(8,128)(2,1)S(1)} %collective-permute-done.1), channel_id=1, source_target_pairs={{0,1},{1,2},{2,3},{3,0},{4,5},{5,6},{6,7},{7,4},{8,9},{9,10},{10,1... | collective-permute-start | bytes 1572872 | tf_op jit(solution)/shard_map/ppermute | solution.py:15
Sparse Core Ops, SparseCore 0:
  8.9 152.3 all-gather.2
  162.8 147.7 all-gather.4
  327.3 29.3 reduce-scatter.1
